TPU v7x, 32 devices: a whole 2x2x4 slice. The times are simulated.
32 devices in a mesh: sp: 8 (over z, y), tp: 4 (over x, core).
Axes of the slice: x: 2, y: 2, z: 4, core: 2. Of those that a mesh axis runs over, the one named last changes fastest.
Arguments:
- residual: bfloat16 [8192, 2048], P('sp'), may hold values from -8 to 8
- query_wide: bfloat16 [8192, 1024], P('sp', 'tp'), may hold values from -6 to 6
- key_wide: bfloat16 [8192, 1024], P('sp', 'tp'), may hold values from -6 to 6
- value_wide: bfloat16 [8192, 2048], P('sp', 'tp'), may hold values from -6 to 6
- decay_wide: bfloat16 [8192, 1024], P('sp', 'tp'), may hold values from -12 to 12
- gate_wide: bfloat16 [8192, 2048], P('sp', 'tp'), may hold values from -6 to 6
- query_narrow: bfloat16 [8192, 512], P('sp', 'tp'), may hold values from -6 to 6
- key_narrow: bfloat16 [8192, 512], P('sp', 'tp'), may hold values from -6 to 6
- value_narrow: bfloat16 [8192, 2048], P('sp', 'tp'), may hold values from -6 to 6
- decay_narrow: bfloat16 [8192, 512], P('sp', 'tp'), may hold values from -12 to 12
- gate_narrow: bfloat16 [8192, 2048], P('sp', 'tp'), may hold values from -6 to 6
- head_gain: float32 [512], replicated, may hold values from 0.1 to 1.9
- out_wide: bfloat16 [2048, 2048], P('tp'), may hold values from -0.125 to 0.125
- out_narrow: bfloat16 [2048, 2048], P('tp'), may hold values from -0.125 to 0.125
- mlp_gain: float32 [2048], replicated, may hold values from 0.1 to 1.9
- up_weight: bfloat16 [2048, 4096], P('sp', 'tp'), may hold values from -0.125 to 0.125
- down_weight: bfloat16 [4096, 2048], P('tp', 'sp'), may hold values from -0.09375 to 0.09375
Outputs:
- layer_out: bfloat16 [8192, 2048], P('sp', 'tp')
All inputs are finite; a program needn't handle non-finite values.
Results may differ from a plain program's by a relative error of at most 0.017.
Values may be sent and summed in bfloat16 or wider, within the bound.
A program may use at most 128 MiB of HBM per device.

v0:
```python
import jax
import jax.numpy as jnp
from jax import lax
from jax.sharding import PartitionSpec as P

HEADS = 4
BLOCK = 64


EPS = 1e-05
DECAY_NORMALIZER = 16.0
HIGHEST = lax.Precision.HIGHEST


def entering(array, axis, join, neutral):
    place = lax.axis_index(axis)
    gathered = jax.tree.map(
        lambda a, kind: lax.all_gather(a.astype(kind), axis),
        array,
        (jnp.bfloat16, jnp.bfloat16, jnp.bfloat16, jnp.bfloat16),
    )
    state = jax.tree.map(lambda a, e: jnp.zeros_like(a) + jnp.asarray(e, a.dtype), array, neutral)

    def one(step, state):
        return join(
            state,
            jax.tree.map(
                lambda a, own: lax.dynamic_index_in_dim(a, step, 0, False).astype(own.dtype),
                gathered,
                array,
            ),
        )

    return lax.fori_loop(0, place, one, state)


def block_pass(queries, keys_in, values_in, log_decay, block_len):
    num_blocks = queries.shape[0] // block_len

    def to_blocks(stacked):
        return stacked.reshape((num_blocks, block_len) + stacked.shape[1:])

    causal = jnp.tril(jnp.ones((block_len, block_len), dtype=bool))
    initial = (
        jnp.zeros((queries.shape[1], queries.shape[2], values_in.shape[2]), jnp.float32),
        jnp.zeros((queries.shape[1], queries.shape[2]), jnp.float32),
    )

    def advance(running, inputs):
        memory, offset = running
        block_q, block_k, block_v, block_g = inputs
        within = jnp.cumsum(block_g, axis=0)
        final_log = within[-1]
        scaled_q = block_q * jnp.exp(within)
        scaled_k = block_k * jnp.exp(-within)
        outside = jnp.einsum("ihd,hde->ihe", scaled_q, memory, precision=HIGHEST)
        scores = jnp.einsum("ihd,jhd->hij", scaled_q, scaled_k, precision=HIGHEST)
        scores = jnp.where(causal[None], scores, 0.0)
        inside = jnp.einsum("hij,jhe->ihe", scores, block_v, precision=HIGHEST)
        decayed_keys = scaled_k * jnp.exp(final_log)[None]
        memory = jnp.exp(final_log)[..., None] * memory + jnp.einsum(
            "jhd,jhe->hde", decayed_keys, block_v, precision=HIGHEST
        )
        carried_q = scaled_q * jnp.exp(offset)[None]
        return ((memory, offset + final_log), (outside + inside, carried_q))

    (memory, totals), (outputs, carried_q) = lax.scan(
        advance,
        initial,
        (to_blocks(queries), to_blocks(keys_in), to_blocks(values_in), to_blocks(log_decay)),
    )
    return (outputs.reshape(values_in.shape), carried_q.reshape(queries.shape), totals, memory)


def prepare(query, key_proj, value, decay, heads_here):
    row_count = query.shape[0]
    key_width = query.shape[1] // heads_here
    queries = query.astype(jnp.float32).reshape(row_count, heads_here, key_width) * key_width ** (
        -0.5
    )
    keys_in = key_proj.astype(jnp.float32).reshape(row_count, heads_here, key_width)
    values_in = value.astype(jnp.float32).reshape(
        row_count, heads_here, value.shape[1] // heads_here
    )
    log_decay = (
        jax.nn.log_sigmoid(decay.astype(jnp.float32)).reshape(row_count, heads_here, key_width)
        / DECAY_NORMALIZER
    )
    return (queries, keys_in, values_in, log_decay)


def finish(outputs, gate, head_gain):
    scale = lax.rsqrt(jnp.mean(jnp.square(outputs), axis=-1, keepdims=True) + EPS)
    gated = (
        outputs * scale * head_gain * jax.nn.silu(gate.astype(jnp.float32).reshape(outputs.shape))
    )
    return gated.reshape(outputs.shape[0], -1).astype(jnp.bfloat16)


def combine_states(earlier, later):
    return (
        earlier[0] + later[0],
        jnp.exp(later[0])[..., None] * earlier[1] + later[1],
        earlier[2] + later[2],
        jnp.exp(later[2])[..., None] * earlier[3] + later[3],
    )


def body(
    residual,
    query_wide,
    key_wide,
    value_wide,
    decay_wide,
    gate_wide,
    query_narrow,
    key_narrow,
    value_narrow,
    decay_narrow,
    gate_narrow,
    head_gain,
    out_wide,
    out_narrow,
    mlp_gain,
    up_weight,
    down_weight,
):
    heads_here = HEADS // lax.axis_size("tp")
    up_whole, down_whole = (
        lax.all_gather(up_weight, "sp", axis=0, tiled=True),
        lax.all_gather(down_weight, "sp", axis=1, tiled=True),
    )
    wq, wk, wv, wg = prepare(query_wide, key_wide, value_wide, decay_wide, heads_here)
    wide_out, wide_q, wide_total, wide_memory = block_pass(wq, wk, wv, wg, BLOCK)
    nq, nk, nv, ng = prepare(query_narrow, key_narrow, value_narrow, decay_narrow, heads_here)
    narrow_out, narrow_q, narrow_total, narrow_memory = block_pass(nq, nk, nv, ng, BLOCK)
    identity = (
        jnp.zeros_like(wide_total),
        jnp.zeros_like(wide_memory),
        jnp.zeros_like(narrow_total),
        jnp.zeros_like(narrow_memory),
    )
    incoming = entering(
        (wide_total, wide_memory, narrow_total, narrow_memory), "sp", combine_states, identity
    )
    wide_out = wide_out + jnp.einsum("ihd,hde->ihe", wide_q, incoming[1], precision=HIGHEST)
    narrow_out = narrow_out + jnp.einsum("ihd,hde->ihe", narrow_q, incoming[3], precision=HIGHEST)
    gated_wide = finish(wide_out, gate_wide, head_gain)
    gated_narrow = finish(narrow_out, gate_narrow, head_gain)
    head_terms = jnp.dot(gated_wide, out_wide, preferred_element_type=jnp.float32) + jnp.dot(
        gated_narrow, out_narrow, preferred_element_type=jnp.float32
    )
    tp_index = lax.axis_index("tp")
    col_count = residual.shape[1] // lax.axis_size("tp")
    full_width = residual.shape[1]
    residual_cols = lax.dynamic_slice_in_dim(residual, tp_index * col_count, col_count, 1)
    mixed_cols = lax.psum_scatter(
        head_terms.astype(jnp.bfloat16), "tp", scatter_dimension=1, tiled=True
    ).astype(jnp.float32)
    stream_cols = (residual_cols.astype(jnp.float32) + mixed_cols).astype(jnp.bfloat16)
    stream_f = stream_cols.astype(jnp.float32)
    squares = lax.psum(jnp.sum(jnp.square(stream_f), axis=1, keepdims=True), "tp")
    gain_cols = lax.dynamic_slice_in_dim(mlp_gain, tp_index * col_count, col_count, 0)
    normed_cols = (stream_f * lax.rsqrt(squares / full_width + EPS) * gain_cols).astype(
        jnp.bfloat16
    )
    normed = lax.all_gather(normed_cols, "tp", axis=1, tiled=True)
    before_activation = jnp.dot(normed, up_whole, preferred_element_type=jnp.float32)
    hidden = jnp.square(jax.nn.relu(before_activation)).astype(jnp.bfloat16)
    down_terms = jnp.dot(hidden, down_whole, preferred_element_type=jnp.float32)
    mlp_cols = lax.psum_scatter(
        down_terms.astype(jnp.bfloat16), "tp", scatter_dimension=1, tiled=True
    ).astype(jnp.float32)
    return (stream_cols.astype(jnp.float32) + mlp_cols).astype(jnp.bfloat16)


def solution(mesh):
    return jax.shard_map(
        body,
        mesh=mesh,
        in_specs=(
            P("sp", None),
            P("sp", "tp"),
            P("sp", "tp"),
            P("sp", "tp"),
            P("sp", "tp"),
            P("sp", "tp"),
            P("sp", "tp"),
            P("sp", "tp"),
            P("sp", "tp"),
            P("sp", "tp"),
            P("sp", "tp"),
            P(),
            P("tp", None),
            P("tp", None),
            P(),
            P("sp", "tp"),
            P("tp", "sp"),
        ),
        out_specs=P("sp", "tp"),
        check_vma=False,
    )
```

profile of v0, /device:TPU:0, one launch (start us, length us, event | category | flops | bytes accessed | tf_op | source)
XLA Modules:
  0.0 591.7 jit_solution(7153783925277661843)
XLA Ops:
  6.6 5.0 reshape.501
  15.4 68.5 %while.51 = (s32[]{:T(128)}, f32[1,128,512]{2,1,0:T(8,128)S(1)}, f32[1,128]{1,0:T(1,128)S(1)}, f32[16,64,1,512]{3,1,2,0:T(8,128)}, f32[16,64,1,128]{3,1,2,0:T(8,...) while((s32[]{:T(128)}, f32[1,128,512]{2,1,0:T(8,128)S(1)}, ...), condition=%wide.region_5.6_spmd.clone, body=%wide.region_3.5_spmd.clone.sunk | while | flops 133005568 | bytes 2333321 | solution.py:67
  84.7 2.7 fusion.81
  87.3 3.3 reshape.486
  91.6 3.3 reshape.487
  95.0 4.9 reshape.499
  99.8 2.0 reshape.498
  103.4 108.7 %while.50 = (s32[]{:T(128)}, f32[1,256,512]{2,1,0:T(8,128)S(1)}, f32[1,256]{1,0:T(1,128)S(1)}, f32[16,64,1,512]{3,1,2,0:T(8,128)}, f32[16,64,1,256]{3,1,2,0:T(8,...) while((s32[]{:T(128)}, f32[1,256,512]{2,1,0:T(8,128)S(1)}, ...), condition=%wide.region_2.3_spmd.clone, body=%wide.region_0.2_spmd.clone.sunk | while | flops 240787968 | bytes 3648133 | solution.py:67
  212.9 3.0 copy.32
  217.2 3.0 copy.34
  221.5 22.3 %all-gather.5 = bf16[8,1,128]{2,1,0:T(2,128)(2,1)S(1)} all-gather(bf16[1,1,128]{2,1,0:T(2,128)(2,1)S(1)} %convert_bitcast_fusion.1), channel_id=4, replica_groups=mesh['sp'=8,'tp'=4] {'sp'}, dimensions={0}, use_global_device_ids=true | all-gather | bytes 2304 | tf_op jit(solution)/shard_map/all_gather | solution.py:18
  243.9 16.7 %all-gather.4 = bf16[8,1,256]{2,1,0:T(2,128)(2,1)S(1)} all-gather(bf16[1,1,256]{2,1,0:T(2,128)(2,1)S(1)} %convert_bitcast_fusion), channel_id=2, replica_groups=mesh['sp'=8,'tp'=4] {'sp'}, dimensions={0}, use_global_device_ids=true | all-gather | bytes 4608 | tf_op jit(solution)/shard_map/all_gather | solution.py:18
  260.6 4.6 all-gather.18.cloned.1.call-done
  265.4 5.6 multiply_reduce_fusion.1
  273.2 2.8 fusion.78
  276.0 5.0 add_convert_fusion
  283.0 56.4 %reduce-scatter.3.cloned.1.call-done = bf16[1024,512]{1,0:T(8,128)(2,1)} async-done(((bf16[1024,2048]{1,0:T(8,128)(2,1)}), bf16[1024,512]{1,0:T(8,128)(2,1)}) %reduce-scatter.3.cloned.1.call-update) | async-done | bytes 1048592 | tf_op jit(solution)/shard_map/reduce_scatter | solution.py:157
  341.4 5.8 psum.7
  348.8 65.5 %all-gather.14.cloned.1.call-done = bf16[2048,1024]{1,0:T(8,128)(2,1)} async-done(((bf16[256,1024]{1,0:T(8,128)(2,1)}), bf16[2048,1024]{1,0:T(8,128)(2,1)}) %all-gather.14.cloned.1.call-update) | async-done | bytes 4194320 | tf_op jit(solution)/shard_map/all_gather | solution.py:130
  414.3 75.1 %all-gather.16.cloned.1.call-done = bf16[1024,2048]{1,0:T(8,128)(2,1)} async-done(((bf16[1024,256]{1,0:T(8,128)(2,1)}), bf16[1024,2048]{1,0:T(8,128)(2,1)}) %all-gather.16.cloned.1.call-update) | async-done | bytes 4194320 | tf_op jit(solution)/shard_map/all_gather | solution.py:131
  489.4 34.1 %all-gather.12.cloned.1.call-done = bf16[1024,2048]{1,0:T(8,128)(2,1)} async-done(((bf16[1024,512]{1,0:T(8,128)(2,1)}), bf16[1024,2048]{1,0:T(8,128)(2,1)}) %all-gather.12.cloned.1.call-update) | async-done | bytes 4194320 | tf_op jit(solution)/shard_map/all_gather | solution.py:167
  523.4 14.4 %convolution_convert_fusion = bf16[1024,2048]{1,0:T(8,128)(2,1)} fusion(bf16[1024,2048]{1,0:T(8,128)(2,1)} %all-gather.16.cloned.1.call-done, bf16[1024,2048]{1,0:T(8,128)(2,1)} %all-gather.12.cloned.1.call-done, bf16[2048,1024]{1,0:T(8,128)(2,1)} %all-gather.14.cloned.1.call-done), kind=kOutput, calls=%fused_computation.91 | convolution fusion | flops 8595177472 | bytes 16777216 | tf_op jit(solution)/shard_map/dot_general | solution.py:170
  537.9 44.5 %reduce-scatter.5.cloned.1.call-done = bf16[1024,512]{1,0:T(8,128)(2,1)} async-done(((bf16[1024,2048]{1,0:T(8,128)(2,1)}), bf16[1024,512]{1,0:T(8,128)(2,1)}) %reduce-scatter.5.cloned.1.call-update) | async-done | bytes 1048592 | tf_op jit(solution)/shard_map/reduce_scatter | solution.py:171
  582.4 2.5 fusion.74
  (423 shorter events, 193.9 us)
Async XLA Ops:
  6.5 266.6 %copy-start = (bf16[512,2048]{1,0:T(8,128)(2,1)S(1)}, bf16[512,2048]{1,0:T(8,128)(2,1)}, u32[]{:S(2)}) copy-start(bf16[512,2048]{1,0:T(8,128)(2,1)} %param.35) | copy-start | bytes 6291460
  6.5 5.0 copy-start.10
  6.5 5.1 copy-start.11
  6.5 254.0 %all-gather.20.cloned.1.call-start = ((), (), s32[]{:S(2)}) async-start(), calls=%async_computation.8 | async-start | bytes 1179648 | tf_op jit(solution)/shard_map/all_gather | solution.py:18
  83.9 6.7 %copy-start.7 = (bf16[1024,256]{1,0:T(8,128)(2,1)S(1)}, bf16[1024,256]{1,0:T(8,128)(2,1)}, u32[]{:S(2)}) copy-start(bf16[1024,256]{1,0:T(8,128)(2,1)} %param.24) | copy-start | bytes 1572868
  84.6 180.5 %all-gather.18.cloned.1.call-start = ((), (), s32[]{:S(2)}) async-start(), calls=%async_computation.7 | async-start | bytes 2359296 | tf_op jit(solution)/shard_map/all_gather | solution.py:18
  91.6 8.2 %copy-start.8 = (bf16[1024,256]{1,0:T(8,128)(2,1)S(1)}, bf16[1024,256]{1,0:T(8,128)(2,1)}, u32[]{:S(2)}) copy-start(bf16[1024,256]{1,0:T(8,128)(2,1)} %param.25) | copy-start | bytes 1572868
  212.9 126.6 %reduce-scatter.3.cloned.1.call-start = ((), (), s32[]{:S(2)}) async-start(), calls=%async_computation.2 | async-start | bytes 5242880 | tf_op jit(solution)/shard_map/reduce_scatter | solution.py:157
  212.9 3.0 copy-start.3
  217.2 3.0 copy-start.4
  265.4 5.7 copy-start.2
  265.4 5.7 copy-start.9
  271.1 2.1 copy-start.6
  271.1 2.1 copy-start.13
  273.2 2.8 copy-start.5
  273.2 2.8 copy-start.12
  281.0 133.2 %all-gather.14.cloned.1.call-start = ((), (), s32[]{:S(2)}) async-start(), calls=%async_computation.4 | async-start | bytes 4718592 | tf_op jit(solution)/shard_map/all_gather | solution.py:130
  281.6 207.7 %all-gather.16.cloned.1.call-start = ((), (), s32[]{:S(2)}) async-start(), calls=%async_computation.5 | async-start | bytes 4718592 | tf_op jit(solution)/shard_map/all_gather | solution.py:131
  282.2 241.2 %all-gather.12.cloned.1.call-start = ((), (), s32[]{:S(2)}) async-start(), calls=%async_computation.3 | async-start | bytes 5242880 | tf_op jit(solution)/shard_map/all_gather | solution.py:167
  348.5 233.9 %reduce-scatter.5.cloned.1.call-start = ((), (), s32[]{:S(2)}) async-start(), calls=%async_computation.6 | async-start | bytes 5242880 | tf_op jit(solution)/shard_map/reduce_scatter | solution.py:171
  537.9 47.0 %copy-start.1 = (bf16[512,2048]{1,0:T(8,128)(2,1)S(1)}, bf16[512,2048]{1,0:T(8,128)(2,1)}, u32[]{:S(2)}) copy-start(bf16[512,2048]{1,0:T(8,128)(2,1)} %param.35) | copy-start | bytes 6291460
Sparse Core Ops, SparseCore 0:
  84.7 43.0 all-gather.19
  213.0 52.1 all-gather.17
  281.2 58.2 reduce-scatter.2
  341.4 72.7 all-gather.13
  416.2 73.1 all-gather.15
  490.8 32.6 all-gather.11
  538.0 44.3 reduce-scatter.4
where the time goes:
time: 596 us; the launch traced here: 592 us
  waiting for transfers between devices  281 us (47%)
  matrix products  95.3 us (16%)
  local copies, waits for them, and re-layouts  83 us (14%)
  other arithmetic  71.2 us (12%)
  blocking collectives  44.8 us (8%)
  between operations  13.8 us (2%)
    all_gather x1, waiting for transfers between devices, body(): lax.all_gather(down_weight, 'sp', axis=1, tiled=True)  75.1 us
    all_gather x1, waiting for transfers between devices, body(): lax.all_gather(up_weight, 'sp', axis=0, tiled=True)  65.5 us
    reduce_scatter x1, waiting for transfers between devices, body(): lax.psum_scatter(head_terms.astype(jnp.bfloat16), 'tp', scatter_dimension...  56.4 us
    reduce_scatter x1, waiting for transfers between devices, body(): lax.psum_scatter(down_terms.astype(jnp.bfloat16), 'tp', scatter_dimension...  44.5 us
    dynamic_slice x48, local copies, waits for them, and re-layouts, block_pass(): lax.scan(advance, initial, (to_blocks(queries), to_blocks(keys_in), to_bl...  41.7 us
    all_gather x2, blocking collectives, entering(): lax.all_gather(a.astype(kind), axis)  39 us
    all_gather x1, waiting for transfers between devices, body(): normed = lax.all_gather(normed_cols, 'tp', axis=1, tiled=True)  34.1 us
    dot_general x32, matrix products, advance(): outside = jnp.einsum('ihd,hde->ihe', scaled_q, memory, precision=HIGHEST)  22.1 us
  transfers between devices with their start and end apart: 7, of which 6 were waited for; matrix products, arithmetic and copies ran while one was open for 24% of the time, Pallas kernels for 0%

commit v1 on v0

v1 whole, which is shorter than its diff:
```python
import functools
import jax
import jax.numpy as jnp
from jax import lax
from jax.experimental import pallas as pl
from jax.experimental.pallas import tpu as pltpu
from jax.sharding import PartitionSpec as P

HEADS = 4
EPS = 1e-05
DECAY_NORMALIZER = 16.0
MESH = pl.DeviceIdType.MESH
BF = jnp.bfloat16
F32 = jnp.float32
VM = pltpu.VMEM


def vmem():
    return pl.BlockSpec(memory_space=VM)


def dot(a, b, dims):
    return lax.dot_general(a, b, (dims, ((), ())), preferred_element_type=F32)


NT = ((1,), (1,))
NN = ((1,), (0,))
TN = ((0,), (0,))


def local_group(q, k, v, d, out, carried, memory, offset, tril, scale):
    rows = q.shape[0]
    decay = d[...].astype(F32)
    g = (jnp.minimum(decay, 0.0) - jnp.log1p(jnp.exp(-jnp.abs(decay)))) / DECAY_NORMALIZER
    high = g.astype(BF)
    low = (g - high.astype(F32)).astype(BF)
    ones = tril.astype(F32).astype(BF)
    within = dot(ones, high, NN) + dot(ones, low, NN)
    mid = within[rows // 2 - 1 : rows // 2]
    last = within[rows - 1 : rows]
    scaled_q = q[...].astype(F32) * scale * jnp.exp(within - mid)
    scaled_k = k[...].astype(F32) * jnp.exp(mid - within)
    value = v[...]
    scores = dot(scaled_q.astype(BF), scaled_k.astype(BF), NT)
    scores = jnp.where(tril, scores, 0.0).astype(BF)
    whole_q = scaled_q * jnp.exp(mid)
    state = memory[...]
    out[...] = (dot(scores, value, NN) + dot(whole_q.astype(BF), state.astype(BF), NT)).astype(
        out.dtype
    )
    carried[...] = (whole_q * jnp.exp(offset[...])).astype(BF)
    keys = (scaled_k * jnp.exp(last - mid)).astype(BF)
    memory[...] = state * jnp.exp(last) + dot(value, keys, TN)
    offset[...] = offset[...] + last


def local_kernel(
    qw, kw, vw, dw, qn, kn, vn, dn, ow, cw, on, cn, packed, mw, mn, fw, fn
):
    step = pl.program_id(0)
    rows = qw.shape[0]

    @pl.when(step == 0)
    def _():
        for ref in (mw, mn, fw, fn):
            ref[...] = jnp.zeros_like(ref)

    tril = lax.broadcasted_iota(jnp.int32, (rows, rows), 0) >= lax.broadcasted_iota(
        jnp.int32, (rows, rows), 1
    )
    local_group(qw, kw, vw, dw, ow, cw, mw, fw, tril, qw.shape[1] ** -0.5)
    local_group(qn, kn, vn, dn, on, cn, mn, fn, tril, qn.shape[1] ** -0.5)

    @pl.when(step == pl.num_programs(0) - 1)
    def _():
        wide, values = qw.shape[1], vw.shape[1]
        packed[:values, :wide] = mw[...].astype(BF)
        packed[:values, wide:] = mn[...].astype(BF)
        extra = packed.shape[0] - values
        packed[values:, :wide] = jnp.broadcast_to(jnp.exp(fw[...]), (extra, wide)).astype(BF)
        packed[values:, wide:] = jnp.broadcast_to(
            jnp.exp(fn[...]), (extra, qn.shape[1])
        ).astype(BF)


def local_pass(qw, kw, vw, dw, qn, kn, vn, dn):
    tokens, wide = qw.shape
    narrow, values = qn.shape[1], vw.shape[1]
    rows = min(128, tokens)

    def spec(width):
        return pl.BlockSpec((rows, width), lambda i: (i, 0))

    whole = (values + 16, wide + narrow)
    return pl.pallas_call(
        local_kernel,
        grid=(tokens // rows,),
        in_specs=[spec(x.shape[1]) for x in (qw, kw, vw, dw, qn, kn, vn, dn)],
        out_specs=[
            spec(values), spec(wide), spec(values), spec(narrow),
            pl.BlockSpec(whole, lambda i: (0, 0)),
        ],
        out_shape=[
            jax.ShapeDtypeStruct((tokens, values), BF),
            jax.ShapeDtypeStruct((tokens, wide), BF),
            jax.ShapeDtypeStruct((tokens, values), BF),
            jax.ShapeDtypeStruct((tokens, narrow), BF),
            jax.ShapeDtypeStruct(whole, BF),
        ],
        scratch_shapes=[
            VM((values, wide), F32), VM((values, narrow), F32),
            VM((1, wide), F32), VM((1, narrow), F32),
        ],
        cost_estimate=pl.CostEstimate(
            flops=30 * 10**9, bytes_accessed=12 * 2**20, transcendentals=0
        ),
        name="local_pass",
    )(qw, kw, vw, dw, qn, kn, vn, dn)


def ring_kernel(n, mine, every, send_sem, recv_sem):
    s = lax.axis_index("sp")
    half = n // 2

    def index_of(p):
        p = lax.rem(p + n, n)
        return jnp.where(p < half, 2 * p, 2 * (n - 1 - p) + 1)

    place = jnp.where(lax.rem(s, 2) == 0, s // 2, n - (s + 1) // 2)
    sides = (index_of(place + 1), index_of(place - 1))
    barrier = pltpu.get_barrier_semaphore()
    for side in sides:
        pl.semaphore_signal(barrier, inc=1, device_id={"sp": side}, device_id_type=MESH)
    pl.semaphore_wait(barrier, 2)
    cut = mine.shape[0] // 32 * 16
    pieces = (pl.ds(0, cut), pl.ds(cut, mine.shape[0] - cut))
    copies = {}
    for far in range(1, half + 1):
        for piece in (0, 1):
            for way in (0, 1):
                if far == half and piece != way:
                    continue
                origin = index_of(place - (far - 1) if way == 0 else place + (far - 1))
                if far > 1:
                    copies[far - 1, piece, way].wait_recv()
                    source = every.at[origin, pieces[piece]]
                else:
                    source = mine.at[pieces[piece]]
                copy = pltpu.make_async_remote_copy(
                    src_ref=source,
                    dst_ref=every.at[origin, pieces[piece]],
                    send_sem=send_sem.at[way, far - 1, piece],
                    recv_sem=recv_sem.at[way, far - 1, piece],
                    device_id={"sp": sides[way]},
                    device_id_type=MESH,
                )
                copy.start()
                copies[far, piece, way] = copy
    every[s] = mine[...]
    for (far, piece, way), copy in copies.items():
        copy.wait_send()
        if far == half or (far == half - 1 and piece != way):
            copy.wait_recv()


def ring(packed, n):
    return pl.pallas_call(
        functools.partial(ring_kernel, n),
        out_shape=jax.ShapeDtypeStruct((n,) + packed.shape, BF),
        in_specs=[vmem()],
        out_specs=vmem(),
        scratch_shapes=[
            pltpu.SemaphoreType.DMA((2, n // 2, 2)),
            pltpu.SemaphoreType.DMA((2, n // 2, 2)),
        ],
        compiler_params=pltpu.CompilerParams(collective_id=0, has_side_effects=True),
        cost_estimate=pl.CostEstimate(
            flops=30 * 10**9, bytes_accessed=2**20, transcendentals=0
        ),
        name="state_ring",
    )(packed)


def gated(local, carried, state, gate, gain):
    out = local[...].astype(F32) + dot(carried[...], state, NT)
    scale = lax.rsqrt(jnp.mean(jnp.square(out), axis=-1, keepdims=True) + EPS)
    u = gate[...].astype(F32)
    return (out * scale * gain[...] * (u / (1.0 + jnp.exp(-u)))).astype(BF)


def finish_kernel(every, ow, cw, gw, on, cn, gn, gain, weight_w, weight_n, out, total, state):
    wide = cw.shape[1]
    values = ow.shape[1]

    @pl.when(pl.program_id(0) == 0)
    def _():
        total[...] = jnp.zeros_like(total)

        def one(j, carry):
            decay = every[j, values : values + 16, :].astype(F32)[:1]
            total[...] = total[...] * decay + every[j, :values, :].astype(F32)
            return carry

        lax.fori_loop(0, lax.axis_index("sp"), one, 0)
        state[...] = total[...].astype(BF)

    left = gated(ow, cw, state[:, :wide], gw, gain)
    right = gated(on, cn, state[:, wide:], gn, gain)
    out[...] = (dot(left, weight_w[...], NN) + dot(right, weight_n[...], NN)).astype(BF)


def finish(every, ow, cw, gw, on, cn, gn, gain, weight_w, weight_n):
    tokens, values = ow.shape
    rows = min(256, tokens)
    width = weight_w.shape[1]

    def spec(x):
        return pl.BlockSpec((rows, x.shape[1]), lambda i: (i, 0))

    return pl.pallas_call(
        finish_kernel,
        grid=(tokens // rows,),
        in_specs=[vmem()]
        + [spec(x) for x in (ow, cw, gw, on, cn, gn)]
        + [vmem()] * 3,
        out_specs=pl.BlockSpec((rows, width), lambda i: (i, 0)),
        out_shape=jax.ShapeDtypeStruct((tokens, width), BF),
        scratch_shapes=[
            VM((values, every.shape[2]), F32),
            VM((values, every.shape[2]), BF),
        ],
        compiler_params=pltpu.CompilerParams(vmem_limit_bytes=48 * 2**20),
        cost_estimate=pl.CostEstimate(
            flops=20 * 10**9, bytes_accessed=16 * 2**20, transcendentals=0
        ),
        name="finish",
    )(every, ow, cw, gw, on, cn, gn, gain.reshape(1, -1), weight_w, weight_n)


def remote(src, dst, send, recv, to):
    copy = pltpu.make_async_remote_copy(
        src_ref=src, dst_ref=dst, send_sem=send, recv_sem=recv,
        device_id={"tp": to}, device_id_type=MESH,
    )
    copy.start()
    return copy


def greet(t):
    barrier = pltpu.get_barrier_semaphore()
    near, far = t + 1 - 2 * lax.rem(t, 2), lax.rem(t + 2, 4)
    for other in (near, far):
        pl.semaphore_signal(barrier, inc=1, device_id={"tp": other}, device_id_type=MESH)
    pl.semaphore_wait(barrier, 2)
    return near, far, lax.rem(near + 2, 4)


def reduce_steps(block, chunks, t, near, far, cross, partial, r1, mix, r2, sems, use):
    s1, v1, s2, v2 = sems
    rows = mix.shape[1]
    sent = []
    for which, owner in ((1, cross), (0, near)):
        for c in range(chunks):
            sent.append(
                (which, c, remote(
                    partial.at[block(owner, c)], r1.at[which, c],
                    s1.at[which, c], v1.at[which, c], near,
                ))
            )
    first = {(w, c): x for w, c, x in sent}
    second = []
    for c in range(chunks):
        first[1, c].wait_recv()
        mix[c] = (partial[block(far, c)].astype(F32) + r1[1, c].astype(F32)).astype(BF)
        second.append(remote(mix.at[c], r2.at[c], s2.at[c], v2.at[c], far))
    for c in range(chunks):
        first[0, c].wait_recv()
        second[c].wait_recv()
        use(c, partial[block(t, c)].astype(F32) + r1[0, c].astype(F32) + r2[c].astype(F32))
    return [x for _, _, x in sent] + second


def mix_kernel(
    chunks, partial, residual, gain, stream, normed,
    r1, mix, r2, s1, v1, s2, v2, sx, vx, sn, vn, sf, vf,
):
    t = lax.axis_index("tp")
    near, far, cross = greet(t)
    rows = mix.shape[1]
    own = rows * chunks

    def block(owner, c):
        return pl.ds(pl.multiple_of(owner * own + c * rows, rows), rows), slice(None)

    def norm(where):
        x = stream[where].astype(F32)
        scale = lax.rsqrt(jnp.mean(jnp.square(x), axis=1, keepdims=True) + EPS)
        normed[where] = (x * scale * gain[...]).astype(BF)

    across, beside, relayed = [], [], []

    def use(c, value):
        where = block(t, c)
        stream[where] = (residual[pl.ds(c * rows, rows), :].astype(F32) + value).astype(BF)
        across.append(remote(stream.at[where], stream.at[where], sx.at[c], vx.at[c], far))
        beside.append(remote(stream.at[where], stream.at[where], sn.at[c], vn.at[c], near))

    started = reduce_steps(
        block, chunks, t, near, far, cross, partial, r1, mix, r2, (s1, v1, s2, v2), use
    )
    for c in range(chunks):
        norm(block(t, c))
        beside[c].wait_recv()
        norm(block(near, c))
    for c in range(chunks):
        across[c].wait_recv()
        where = block(far, c)
        relayed.append(remote(stream.at[where], stream.at[where], sf.at[c], vf.at[c], near))
        norm(where)
    for c in range(chunks):
        relayed[c].wait_recv()
        norm(block(cross, c))
    for copy in started + across + beside + relayed:
        copy.wait_send()


def mix_rows(partial, residual, gain):
    tokens, width = partial.shape
    chunks = 4
    rows = tokens // 4 // chunks
    dma = pltpu.SemaphoreType.DMA
    return pl.pallas_call(
        functools.partial(mix_kernel, chunks),
        out_shape=[jax.ShapeDtypeStruct((tokens, width), BF)] * 2,
        in_specs=[vmem()] * 3,
        out_specs=[vmem()] * 2,
        scratch_shapes=[
            VM((2, chunks, rows, width), BF), VM((chunks, rows, width), BF),
            VM((chunks, rows, width), BF),
            dma((2, chunks)), dma((2, chunks)),
        ] + [dma((chunks,))] * 8,
        compiler_params=pltpu.CompilerParams(
            collective_id=1, has_side_effects=True, vmem_limit_bytes=48 * 2**20
        ),
        cost_estimate=pl.CostEstimate(
            flops=50 * 10**9, bytes_accessed=16 * 2**20, transcendentals=0
        ),
        name="mix_rows",
    )(partial, residual, gain.reshape(1, -1))


def last_kernel(chunks, partial, stream, out, r1, mix, r2, s1, v1, s2, v2):
    t = lax.axis_index("tp")
    near, far, cross = greet(t)
    rows, width = mix.shape[1:]

    def block(owner, c):
        return pl.ds(c * rows, rows), pl.ds(pl.multiple_of(owner * width, width), width)

    def use(c, value):
        where = pl.ds(c * rows, rows)
        out[where, :] = (stream[where, :].astype(F32) + value).astype(BF)

    for copy in reduce_steps(
        block, chunks, t, near, far, cross, partial, r1, mix, r2, (s1, v1, s2, v2), use
    ):
        copy.wait_send()


def last_columns(partial, stream):
    tokens, width = stream.shape
    chunks = 4
    rows = tokens // chunks
    dma = pltpu.SemaphoreType.DMA
    return pl.pallas_call(
        functools.partial(last_kernel, chunks),
        out_shape=jax.ShapeDtypeStruct((tokens, width), BF),
        in_specs=[vmem()] * 2,
        out_specs=vmem(),
        scratch_shapes=[
            VM((2, chunks, rows, width), BF), VM((chunks, rows, width), BF),
            VM((chunks, rows, width), BF),
            dma((2, chunks)), dma((2, chunks)), dma((chunks,)), dma((chunks,)),
        ],
        compiler_params=pltpu.CompilerParams(
            collective_id=2, has_side_effects=True, vmem_limit_bytes=32 * 2**20
        ),
        name="last_columns",
    )(partial, stream)


def body(
    residual,
    query_wide,
    key_wide,
    value_wide,
    decay_wide,
    gate_wide,
    query_narrow,
    key_narrow,
    value_narrow,
    decay_narrow,
    gate_narrow,
    head_gain,
    out_wide,
    out_narrow,
    mlp_gain,
    up_weight,
    down_weight,
):
    n_sp, n_tp = lax.axis_size("sp"), lax.axis_size("tp")
    assert n_tp == HEADS == 4 and n_sp % 2 == 0
    up_whole = lax.all_gather(up_weight, "sp", axis=0, tiled=True)
    down_whole = lax.all_gather(down_weight, "sp", axis=1, tiled=True)
    wide_out, wide_q, narrow_out, narrow_q, packed = local_pass(
        query_wide, key_wide, value_wide, decay_wide,
        query_narrow, key_narrow, value_narrow, decay_narrow,
    )
    every = ring(packed, n_sp)
    partial = finish(
        every, wide_out, wide_q, gate_wide, narrow_out, narrow_q, gate_narrow,
        head_gain, out_wide, out_narrow,
    )
    t = lax.axis_index("tp")
    own_rows = residual.shape[0] // n_tp
    own_cols = residual.shape[1] // n_tp
    residual_rows = lax.dynamic_slice_in_dim(residual, t * own_rows, own_rows, 0)
    stream, normed = mix_rows(partial, residual_rows, mlp_gain)
    stream_cols = lax.dynamic_slice_in_dim(stream, t * own_cols, own_cols, 1)
    before = jnp.dot(normed, up_whole, preferred_element_type=F32)
    hidden = jnp.square(jax.nn.relu(before)).astype(BF)
    down_terms = jnp.dot(hidden, down_whole, preferred_element_type=F32).astype(BF)
    return last_columns(down_terms, stream_cols)


def solution(mesh):
    return jax.shard_map(
        body,
        mesh=mesh,
        in_specs=(
            P("sp", None),
            P("sp", "tp"),
            P("sp", "tp"),
            P("sp", "tp"),
            P("sp", "tp"),
            P("sp", "tp"),
            P("sp", "tp"),
            P("sp", "tp"),
            P("sp", "tp"),
            P("sp", "tp"),
            P("sp", "tp"),
            P(),
            P("tp", None),
            P("tp", None),
            P(),
            P("sp", "tp"),
            P("tp", "sp"),
        ),
        out_specs=P("sp", "tp"),
        check_vma=False,
    )
```

time: 596 us -> 234 us (0.39)
  waiting for transfers between devices: 281 us -> 23.8 us
  Pallas kernels: 0 us -> 175 us
  matrix products: 95.3 us -> 14.4 us
  local copies, waits for them, and re-layouts: 83 us -> 6.94 us
  other arithmetic: 71.2 us -> 0 us
  blocking collectives: 44.8 us -> 0 us
    pallas_call x0 -> x5, Pallas kernels: none -> 175 us  [the longest x1 70.1 us: ring(): pl.pallas_call(functools.partial(ring_kernel, n), out_shape=jax.ShapeDtyp...]
    all_gather x5 -> x2, waiting for transfers between devices: 179 us -> 22.4 us  [the longest x1 22.4 us: body(): down_whole = lax.all_gather(down_weight, 'sp', axis=1, tiled=True)]
    reduce_scatter x2 -> x0, waiting for transfers between devices: 101 us -> none  [the longest x1 56.4 us: body(): lax.psum_scatter(head_terms.astype(jnp.bfloat16), 'tp', scatter_dimension...]
    dot_general x133 -> x1, matrix products: 95.3 us -> 14.4 us  [body(): jnp.dot(hidden, down_whole, preferred_element_type=F32).astype(BF)]
    dynamic_slice x49 -> x2, local copies, waits for them, and re-layouts: 42.4 us -> 1.45 us  [the longest x1 1.33 us: body(): lax.dynamic_slice_in_dim(residual, t * own_rows, own_rows, 0)]
    all_gather x2 -> x0, blocking collectives: 39 us -> none  [entering(): lax.all_gather(a.astype(kind), axis)]
    mul x34 -> x0, other arithmetic: 33.1 us -> none  [the longest x16 17 us: advance(): carried_q = scaled_q * jnp.exp(offset)[None]]
    another operation x33 -> x0, other arithmetic: 16.7 us -> none  [the longest x32 15.7 us: advance(): within = jnp.cumsum(block_g, axis=0)]
  transfers between devices with their start and end apart: 7 -> 2, of which waited for: 6 -> 1; matrix products, arithmetic and copies ran while one was open for 24% -> 1% of each run, Pallas kernels for 0% -> 63%
where the time goes in v1:
time: 234 us; the launch traced here: 233 us
  Pallas kernels  175 us (75%)
  waiting for transfers between devices  23.8 us (10%)
  matrix products  14.4 us (6%)
  between operations  13.6 us (6%)
  local copies, waits for them, and re-layouts  6.94 us (3%)
    pallas_call x1, Pallas kernels, ring(): pl.pallas_call(functools.partial(ring_kernel, n), out_shape=jax.ShapeDtyp...  70.1 us
    pallas_call x1, Pallas kernels, mix_rows(): pl.pallas_call(functools.partial(mix_kernel, chunks), out_shape=[jax.Shap...  55.3 us
    pallas_call x1, Pallas kernels, last_columns(): pl.pallas_call(functools.partial(last_kernel, chunks), out_shape=jax.Shap...  27.3 us
    all_gather x1, waiting for transfers between devices, body(): down_whole = lax.all_gather(down_weight, 'sp', axis=1, tiled=True)  22.4 us
    dot_general x1, matrix products, body(): jnp.dot(hidden, down_whole, preferred_element_type=F32).astype(BF)  14.4 us
    pallas_call x1, Pallas kernels, finish(): pl.pallas_call(finish_kernel, grid=(tokens // rows,), in_specs=[vmem()] +...  11.1 us
    pallas_call x1, Pallas kernels, local_pass(): pl.pallas_call(local_kernel, grid=(tokens // rows,), in_specs=[spec(x.sha...  10.9 us
    unnamed x19, local copies, waits for them, and re-layouts  5.48 us
  transfers between devices with their start and end apart: 2, of which 1 were waited for; matrix products, arithmetic and copies ran while one was open for 1% of the time, Pallas kernels for 63%

profile of v1, /device:TPU:0, one launch (start us, length us, event | category | flops | bytes accessed | tf_op | source)
XLA Modules:
  0.0 233.4 jit_solution(8764567972759551136)
XLA Ops:
  6.5 0.0 all-gather.3.cloned.1.call-start
  6.5 0.7 all-gather.3.cloned.1.call-update
  7.3 0.0 all-gather.5.cloned.1.call-start
  7.3 0.7 all-gather.5.cloned.1.call-update
  8.0 10.9 %local_pass.1 = (bf16[1024,512]{1,0:T(8,128)(2,1)}, bf16[1024,256]{1,0:T(8,128)(2,1)}, bf16[1024,512]{1,0:T(8,128)(2,1)}, bf16[1024,128]{1,0:T(8,128)(2,1)}, bf16[528,384]{1,0:T(8,128)(2,1)}) custom-call(bf16[1024,256]{1,0:T(8,128)(2,1)} %qw.1, bf16[1024,256]{1,0:T(8,128)(2,1)} %kw.1, bf16[1024,512]{1,0:T(8,128)(2,1)} %vw.1, bf16[1024,256]{1,0:T(8,128)(2,1)} %dw.1, ...), custom_call_target="tpu_custom_call" | custom-call | flops 30000001024 | bytes 12582912 | tf_op jit(solution)/shard_map/local_pass/pallas_call | solution.py:95
  18.9 0.0 copy-start.1
  18.9 0.0 copy-start.2
  18.9 0.0 copy-start.4
  18.9 0.0 copy-start.5
  18.9 0.0 copy-start.8
  18.9 70.1 %state_ring.1.every = bf16[8,528,384]{2,1,0:T(8,128)(2,1)} custom-call(bf16[528,384]{1,0:T(8,128)(2,1)} %get-tuple-element.12.mine), custom_call_target="tpu_custom_call" | custom-call | flops 30000001024 | bytes 1048576 | tf_op jit(solution)/shard_map/state_ring/pallas_call | solution.py:167
  89.0 1.3 constant_dynamic-slice_fusion.1.residual
  90.4 1.2 copy-done.6
  91.6 1.1 copy-done.7
  92.7 11.1 %finish.1.partial = bf16[1024,2048]{1,0:T(8,128)(2,1)} custom-call(bf16[8,528,384]{2,1,0:T(8,128)(2,1)} %state_ring.1.every, bf16[1024,512]{1,0:T(8,128)(2,1)S(1)} %copy-done.5, bf16[1024,256]{1,0:T(8,128)(2,1)S(1)} %copy-done.7, bf16[1024,512]{1,0:T(8,128)(2,1)S(1)} %copy-done.1, bf16[1024,512]{1,0:T(8,128)(2,1)S(1)} %copy-done.6, ...), custom_call_target="tpu_custom_call" | custom-call | flops 20000000000 | bytes 16777216 | tf_op jit(solution)/shard_map/finish/pallas_call | solution.py:220
  103.8 0.0 copy-done.3
  103.8 55.3 %mix_rows.1 = (bf16[1024,2048]{1,0:T(8,128)(2,1)S(1)}, bf16[1024,2048]{1,0:T(8,128)(2,1)}) custom-call(bf16[1024,2048]{1,0:T(8,128)(2,1)} %finish.1.partial, bf16[256,2048]{1,0:T(8,128)(2,1)S(1)} %constant_dynamic-slice_fusion.1.residual, f32[1,2048]{1,0:T(1,128)S(1)} %bitcast.5), custom_call_target="tpu_custom_call" | custom-call | flops 49999998976 | bytes 16777216 | tf_op jit(solution)/shard_map/mix_rows/pallas_call | solution.py:332
  159.1 0.1 constant_dynamic-slice_fusion.stream
  159.3 0.0 all-gather.3.cloned.1.call-done
  159.3 22.4 %all-gather.5.cloned.1.call-done = bf16[1024,2048]{1,0:T(8,128)(2,1)} async-done(((bf16[1024,256]{1,0:T(8,128)(2,1)}), bf16[1024,2048]{1,0:T(8,128)(2,1)}) %all-gather.5.cloned.1.call-update) | async-done | bytes 4194320 | tf_op jit(solution)/shard_map/all_gather | solution.py:414
  181.7 14.4 %convolution_convert_fusion.partial = bf16[1024,2048]{1,0:T(8,128)(2,1)} fusion(bf16[1024,2048]{1,0:T(8,128)(2,1)} %all-gather.5.cloned.1.call-done, bf16[1024,2048]{1,0:T(8,128)(2,1)} %get-tuple-element.17, bf16[2048,1024]{1,0:T(8,128)(2,1)} %all-gather.3.cloned.1.call-done), kind=kOutput, calls=%fused_computation.1 | convolution fusion | flops 8595177472 | bytes 16777216 | tf_op jit(solution)/shard_map/dot_general | solution.py:432
  196.0 2.2 copy-done
  198.2 27.3 %last_columns.1 = bf16[1024,512]{1,0:T(8,128)(2,1)S(1)} custom-call(bf16[1024,2048]{1,0:T(8,128)(2,1)S(1)} %copy-done, bf16[1024,512]{1,0:T(8,128)(2,1)S(1)} %constant_dynamic-slice_fusion.stream), custom_call_target="tpu_custom_call" | custom-call | tf_op jit(solution)/shard_map/last_columns/pallas_call | solution.py:375
  225.6 1.0 copy.19
  (9 shorter events, 0.0 us)
Async XLA Ops:
  6.5 152.8 %all-gather.3.cloned.1.call-start = ((), (), s32[]{:S(2)}) async-start(), calls=%async_computation | async-start | bytes 4718592 | tf_op jit(solution)/shard_map/all_gather | solution.py:413
  7.3 174.4 %all-gather.5.cloned.1.call-start = ((), (), s32[]{:S(2)}) async-start(), calls=%async_computation.1 | async-start | bytes 4718592 | tf_op jit(solution)/shard_map/all_gather | solution.py:414
  18.9 71.5 %copy-start.1 = (bf16[1024,512]{1,0:T(8,128)(2,1)S(1)}, bf16[1024,512]{1,0:T(8,128)(2,1)}, u32[]{:S(2)}) copy-start(bf16[1024,512]{1,0:T(8,128)(2,1)} %gw.1) | copy-start | bytes 3145732
  18.9 71.5 %copy-start.2 = (bf16[1024,512]{1,0:T(8,128)(2,1)S(1)}, bf16[1024,512]{1,0:T(8,128)(2,1)}, u32[]{:S(2)}) copy-start(bf16[1024,512]{1,0:T(8,128)(2,1)} %gn.1) | copy-start | bytes 3145732
  18.9 71.5 %copy-start.4 = (f32[512]{0:T(512)S(1)}, f32[512]{0:T(512)}, u32[]{:S(2)}) copy-start(f32[512]{0:T(512)} %param.28) | copy-start | bytes 6148
  18.9 71.5 %copy-start.5 = (bf16[1024,512]{1,0:T(8,128)(2,1)S(1)}, bf16[1024,512]{1,0:T(8,128)(2,1)}, u32[]{:S(2)}) copy-start(bf16[1024,512]{1,0:T(8,128)(2,1)} %get-tuple-element.13.ow) | copy-start | bytes 3145732
  18.9 71.5 %copy-start.8 = (bf16[1024,128]{1,0:T(8,128)(2,1)S(1)}, bf16[1024,128]{1,0:T(8,128)(2,1)}, u32[]{:S(2)}) copy-start(bf16[1024,128]{1,0:T(8,128)(2,1)} %get-tuple-element.16.cn) | copy-start | bytes 786436
  90.4 1.2 copy-start.6
  91.6 1.1 copy-start.7
  92.7 11.1 %copy-start.3 = (f32[2048]{0:T(1024)S(1)}, f32[2048]{0:T(1024)}, u32[]{:S(2)}) copy-start(f32[2048]{0:T(1024)} %param.31) | copy-start | bytes 24580
  196.0 2.2 copy-start
Sparse Core Ops, SparseCore 0:
  9.5 96.3 all-gather.2
  107.9 73.7 all-gather.4

commit v2 on v1

--- a/solution.py
+++ b/solution.py
@@ -118,7 +118,7 @@
     )(qw, kw, vw, dw, qn, kn, vn, dn)
 
 
-def ring_kernel(n, mine, every, send_sem, recv_sem):
+def ring_place(n):
     s = lax.axis_index("sp")
     half = n // 2
 
@@ -127,40 +127,60 @@
         return jnp.where(p < half, 2 * p, 2 * (n - 1 - p) + 1)
 
     place = jnp.where(lax.rem(s, 2) == 0, s // 2, n - (s + 1) // 2)
-    sides = (index_of(place + 1), index_of(place - 1))
-    barrier = pltpu.get_barrier_semaphore()
-    for side in sides:
-        pl.semaphore_signal(barrier, inc=1, device_id={"sp": side}, device_id_type=MESH)
-    pl.semaphore_wait(barrier, 2)
+    return place, index_of, (index_of(place + 1), index_of(place - 1))
+
+
+def ring_steps(n, mine, every, send_sem, recv_sem):
+    half = n // 2
+    place, index_of, sides = ring_place(n)
     cut = mine.shape[0] // 32 * 16
     pieces = (pl.ds(0, cut), pl.ds(cut, mine.shape[0] - cut))
     copies = {}
-    for far in range(1, half + 1):
-        for piece in (0, 1):
-            for way in (0, 1):
-                if far == half and piece != way:
-                    continue
-                origin = index_of(place - (far - 1) if way == 0 else place + (far - 1))
-                if far > 1:
-                    copies[far - 1, piece, way].wait_recv()
-                    source = every.at[origin, pieces[piece]]
-                else:
-                    source = mine.at[pieces[piece]]
-                copy = pltpu.make_async_remote_copy(
-                    src_ref=source,
-                    dst_ref=every.at[origin, pieces[piece]],
-                    send_sem=send_sem.at[way, far - 1, piece],
-                    recv_sem=recv_sem.at[way, far - 1, piece],
-                    device_id={"sp": sides[way]},
-                    device_id_type=MESH,
-                )
-                copy.start()
-                copies[far, piece, way] = copy
-    every[s] = mine[...]
-    for (far, piece, way), copy in copies.items():
-        copy.wait_send()
-        if far == half or (far == half - 1 and piece != way):
-            copy.wait_recv()
+
+    def hop(far, piece, way):
+        origin = index_of(place - (far - 1) if way == 0 else place + (far - 1))
+        if far > 1:
+            copies[far - 1, piece, way].wait_recv()
+            source = every.at[origin, pieces[piece]]
+        else:
+            source = mine.at[pieces[piece]]
+        copy = pltpu.make_async_remote_copy(
+            src_ref=source,
+            dst_ref=every.at[origin, pieces[piece]],
+            send_sem=send_sem.at[way, far - 1, piece],
+            recv_sem=recv_sem.at[way, far - 1, piece],
+            device_id={"sp": sides[way]},
+            device_id_type=MESH,
+        )
+        copy.start()
+        copies[far, piece, way] = copy
+
+    def close():
+        for (far, piece, way), copy in copies.items():
+            copy.wait_send()
+            if far == half or (far == half - 1 and piece != way):
+                copy.wait_recv()
+
+    hops = [
+        functools.partial(hop, far, piece, way)
+        for far in range(1, half + 1)
+        for piece in (0, 1)
+        for way in (0, 1)
+        if far < half or piece == way
+    ]
+    return hops, close
+
+
+def ring_kernel(n, mine, every, send_sem, recv_sem):
+    barrier = pltpu.get_barrier_semaphore()
+    for side in ring_place(n)[2]:
+        pl.semaphore_signal(barrier, inc=1, device_id={"sp": side}, device_id_type=MESH)
+    pl.semaphore_wait(barrier, 2)
+    hops, close = ring_steps(n, mine, every, send_sem, recv_sem)
+    for hop in hops:
+        hop()
+    every[lax.axis_index("sp")] = mine[...]
+    close()
 
 
 def ring(packed, n):
@@ -246,12 +266,14 @@
     return copy
 
 
-def greet(t):
+def greet(t, sides=()):
     barrier = pltpu.get_barrier_semaphore()
     near, far = t + 1 - 2 * lax.rem(t, 2), lax.rem(t + 2, 4)
     for other in (near, far):
         pl.semaphore_signal(barrier, inc=1, device_id={"tp": other}, device_id_type=MESH)
-    pl.semaphore_wait(barrier, 2)
+    for side in sides:
+        pl.semaphore_signal(barrier, inc=1, device_id={"sp": side}, device_id_type=MESH)
+    pl.semaphore_wait(barrier, 2 + len(sides))
     return near, far, lax.rem(near + 2, 4)
 
 
@@ -281,11 +303,16 @@
 
 
 def mix_kernel(
-    chunks, partial, residual, gain, stream, normed,
-    r1, mix, r2, s1, v1, s2, v2, sx, vx, sn, vn, sf, vf,
+    n, chunks, partial, residual, gain, shard, stream, normed, weight,
+    r1, mix, r2, s1, v1, s2, v2, sx, vx, sn, vn, sf, vf, sw, vw,
 ):
     t = lax.axis_index("tp")
-    near, far, cross = greet(t)
+    near, far, cross = greet(t, ring_place(n)[2])
+    hops, close = ring_steps(n, shard, weight, sw, vw)
+    first = [hop for hop in hops if hop.args[0] == 1]
+    later = [hop for hop in hops if hop.args[0] > 1]
+    for hop in first:
+        hop()
     rows = mix.shape[1]
     own = rows * chunks
 
@@ -304,6 +331,8 @@
         stream[where] = (residual[pl.ds(c * rows, rows), :].astype(F32) + value).astype(BF)
         across.append(remote(stream.at[where], stream.at[where], sx.at[c], vx.at[c], far))
         beside.append(remote(stream.at[where], stream.at[where], sn.at[c], vn.at[c], near))
+        for hop in later[2 * c : 2 * c + 2]:
+            hop()
 
     started = reduce_steps(
         block, chunks, t, near, far, cross, partial, r1, mix, r2, (s1, v1, s2, v2), use
@@ -312,6 +341,9 @@
         norm(block(t, c))
         beside[c].wait_recv()
         norm(block(near, c))
+    weight[lax.axis_index("sp")] = shard[...]
+    for hop in later[2 * chunks :]:
+        hop()
     for c in range(chunks):
         across[c].wait_recv()
         where = block(far, c)
@@ -322,23 +354,25 @@
         norm(block(cross, c))
     for copy in started + across + beside + relayed:
         copy.wait_send()
-
-
-def mix_rows(partial, residual, gain):
+    close()
+
+
+def mix_rows(partial, residual, gain, shard, n):
     tokens, width = partial.shape
     chunks = 4
     rows = tokens // 4 // chunks
     dma = pltpu.SemaphoreType.DMA
     return pl.pallas_call(
-        functools.partial(mix_kernel, chunks),
-        out_shape=[jax.ShapeDtypeStruct((tokens, width), BF)] * 2,
-        in_specs=[vmem()] * 3,
-        out_specs=[vmem()] * 2,
+        functools.partial(mix_kernel, n, chunks),
+        out_shape=[jax.ShapeDtypeStruct((tokens, width), BF)] * 2
+        + [jax.ShapeDtypeStruct((n,) + shard.shape, BF)],
+        in_specs=[vmem()] * 4,
+        out_specs=[vmem()] * 3,
         scratch_shapes=[
             VM((2, chunks, rows, width), BF), VM((chunks, rows, width), BF),
             VM((chunks, rows, width), BF),
             dma((2, chunks)), dma((2, chunks)),
-        ] + [dma((chunks,))] * 8,
+        ] + [dma((chunks,))] * 8 + [dma((2, n // 2, 2))] * 2,
         compiler_params=pltpu.CompilerParams(
             collective_id=1, has_side_effects=True, vmem_limit_bytes=48 * 2**20
         ),
@@ -346,7 +380,7 @@
             flops=50 * 10**9, bytes_accessed=16 * 2**20, transcendentals=0
         ),
         name="mix_rows",
-    )(partial, residual, gain.reshape(1, -1))
+    )(partial, residual, gain.reshape(1, -1), shard)
 
 
 def last_kernel(chunks, partial, stream, out, r1, mix, r2, s1, v1, s2, v2):
@@ -410,7 +444,6 @@
 ):
     n_sp, n_tp = lax.axis_size("sp"), lax.axis_size("tp")
     assert n_tp == HEADS == 4 and n_sp % 2 == 0
-    up_whole = lax.all_gather(up_weight, "sp", axis=0, tiled=True)
     down_whole = lax.all_gather(down_weight, "sp", axis=1, tiled=True)
     wide_out, wide_q, narrow_out, narrow_q, packed = local_pass(
         query_wide, key_wide, value_wide, decay_wide,
@@ -425,7 +458,8 @@
     own_rows = residual.shape[0] // n_tp
     own_cols = residual.shape[1] // n_tp
     residual_rows = lax.dynamic_slice_in_dim(residual, t * own_rows, own_rows, 0)
-    stream, normed = mix_rows(partial, residual_rows, mlp_gain)
+    stream, normed, up_whole = mix_rows(partial, residual_rows, mlp_gain, up_weight, n_sp)
+    up_whole = up_whole.reshape(-1, up_weight.shape[1])
     stream_cols = lax.dynamic_slice_in_dim(stream, t * own_cols, own_cols, 1)
     before = jnp.dot(normed, up_whole, preferred_element_type=F32)
     hidden = jnp.square(jax.nn.relu(before)).astype(BF)

time: 234 us -> 209 us (0.89)
  waiting for transfers between devices: 23.8 us -> 0.73 us
    all_gather x1, waiting for transfers between devices: 22.4 us -> 0.02 us  [body(): down_whole = lax.all_gather(down_weight, 'sp', axis=1, tiled=True)]
    pallas_call x1, Pallas kernels: 70.1 us -> 66.3 us  [ring(): pl.pallas_call(functools.partial(ring_kernel, n), out_shape=jax.ShapeDtyp...]
    unnamed x19 -> x21, local copies, waits for them, and re-layouts: 5.48 us -> 5.46 us
  transfers between devices with their start and end apart: 2 -> 1, of which waited for: 1 -> 0; matrix products, arithmetic and copies ran while one was open for 1% -> 1% of each run, Pallas kernels for 63% -> 70%
where the time goes in v2:
time: 209 us; the launch traced here: 208 us
  Pallas kernels  173 us (83%)
  matrix products  14.4 us (7%)
  between operations  13.5 us (6%)
  local copies, waits for them, and re-layouts  6.92 us (3%)
    pallas_call x1, Pallas kernels, ring(): pl.pallas_call(functools.partial(ring_kernel, n), out_shape=jax.ShapeDtyp...  66.3 us
    pallas_call x1, Pallas kernels, mix_rows(): pl.pallas_call(functools.partial(mix_kernel, n, chunks), out_shape=[jax.S...  57.1 us
    pallas_call x1, Pallas kernels, last_columns(): pl.pallas_call(functools.partial(last_kernel, chunks), out_shape=jax.Shap...  27.3 us
    dot_general x1, matrix products, body(): jnp.dot(hidden, down_whole, preferred_element_type=F32).astype(BF)  14.4 us
    pallas_call x1, Pallas kernels, finish(): pl.pallas_call(finish_kernel, grid=(tokens // rows,), in_specs=[vmem()] +...  11.1 us
    pallas_call x1, Pallas kernels, local_pass(): pl.pallas_call(local_kernel, grid=(tokens // rows,), in_specs=[spec(x.sha...  10.9 us
    unnamed x21, local copies, waits for them, and re-layouts  5.46 us
  transfers between devices with their start and end apart: 1, of which 0 were waited for; matrix products, arithmetic and copies ran while one was open for 1% of the time, Pallas kernels for 70%

profile of v2, /device:TPU:0, one launch (start us, length us, event | category | flops | bytes accessed | tf_op | source)
XLA Modules:
  0.0 208.3 jit_solution(4863955476768468955)
XLA Ops:
  6.5 0.0 all-gather.2.cloned.1.call-start
  6.5 0.7 all-gather.2.cloned.1.call-update
  7.3 10.9 %local_pass.1 = (bf16[1024,512]{1,0:T(8,128)(2,1)}, bf16[1024,256]{1,0:T(8,128)(2,1)}, bf16[1024,512]{1,0:T(8,128)(2,1)}, bf16[1024,128]{1,0:T(8,128)(2,1)}, bf16[528,384]{1,0:T(8,128)(2,1)}) custom-call(bf16[1024,256]{1,0:T(8,128)(2,1)} %qw.1, bf16[1024,256]{1,0:T(8,128)(2,1)} %kw.1, bf16[1024,512]{1,0:T(8,128)(2,1)} %vw.1, bf16[1024,256]{1,0:T(8,128)(2,1)} %dw.1, ...), custom_call_target="tpu_custom_call" | custom-call | flops 30000001024 | bytes 12582912 | tf_op jit(solution)/shard_map/local_pass/pallas_call | solution.py:95
  18.1 0.0 copy-start.1
  18.2 0.0 copy-start.2
  18.2 0.0 copy-start.5
  18.2 0.0 copy-start.6
  18.2 0.0 copy-start.9
  18.2 66.3 %state_ring.1.every = bf16[8,528,384]{2,1,0:T(8,128)(2,1)} custom-call(bf16[528,384]{1,0:T(8,128)(2,1)} %get-tuple-element.13.mine), custom_call_target="tpu_custom_call" | custom-call | flops 30000001024 | bytes 1048576 | tf_op jit(solution)/shard_map/state_ring/pallas_call | solution.py:187
  84.5 1.3 constant_dynamic-slice_fusion.1.residual
  85.9 0.0 copy-done.1
  85.9 0.0 copy-done.2
  85.9 0.0 copy-done.5
  85.9 1.2 copy-done.7
  87.2 1.0 copy-done.8
  88.2 11.1 %finish.1.partial = bf16[1024,2048]{1,0:T(8,128)(2,1)} custom-call(bf16[8,528,384]{2,1,0:T(8,128)(2,1)} %state_ring.1.every, bf16[1024,512]{1,0:T(8,128)(2,1)S(1)} %copy-done.6, bf16[1024,256]{1,0:T(8,128)(2,1)S(1)} %copy-done.8, bf16[1024,512]{1,0:T(8,128)(2,1)S(1)} %copy-done.1, bf16[1024,512]{1,0:T(8,128)(2,1)S(1)} %copy-done.7, ...), custom_call_target="tpu_custom_call" | custom-call | flops 20000000000 | bytes 16777216 | tf_op jit(solution)/shard_map/finish/pallas_call | solution.py:240
  99.3 0.0 copy-done.4
  99.3 57.1 %mix_rows.1 = (bf16[1024,2048]{1,0:T(8,128)(2,1)S(1)}, bf16[1024,2048]{1,0:T(8,128)(2,1)}, bf16[8,256,1024]{2,1,0:T(8,128)(2,1)}) custom-call(bf16[1024,2048]{1,0:T(8,128)(2,1)} %finish.1.partial, bf16[256,2048]{1,0:T(8,128)(2,1)S(1)} %constant_dynamic-slice_fusion.1.residual, f32[1,2048]{1,0:T(1,128)S(1)} %bitcast.6, bf16[256,1024]{1,0:T(8,128)(2,1)S(1)} %copy-done.3), custom_call_target="tpu_custom_call" | custom-call | flops 49999998976 | bytes 16777216 | tf_op jit(solution)/shard_map/mix_rows/pallas_call | solution.py:365
  156.5 0.1 constant_dynamic-slice_fusion.stream
  156.6 0.0 all-gather.2.cloned.1.call-done
  156.6 14.4 %convolution_convert_fusion.partial = bf16[1024,2048]{1,0:T(8,128)(2,1)} fusion(bf16[1024,2048]{1,0:T(8,128)(2,1)} %all-gather.2.cloned.1.call-done, bf16[1024,2048]{1,0:T(8,128)(2,1)} %get-tuple-element.18, bf16[2048,1024]{1,0:T(8,128)(2,1)} %bitcast.8), kind=kOutput, calls=%fused_computation.1 | convolution fusion | flops 8595177472 | bytes 16777216 | tf_op jit(solution)/shard_map/dot_general | solution.py:466
  171.0 2.2 %copy-done = bf16[1024,2048]{1,0:T(8,128)(2,1)S(1)} copy-done((bf16[1024,2048]{1,0:T(8,128)(2,1)S(1)}, bf16[1024,2048]{1,0:T(8,128)(2,1)}, u32[]{:S(2)}) %copy-start) | copy-done | bytes 4194328
  173.2 27.3 %last_columns.1 = bf16[1024,512]{1,0:T(8,128)(2,1)S(1)} custom-call(bf16[1024,2048]{1,0:T(8,128)(2,1)S(1)} %copy-done, bf16[1024,512]{1,0:T(8,128)(2,1)S(1)} %constant_dynamic-slice_fusion.stream), custom_call_target="tpu_custom_call" | custom-call | tf_op jit(solution)/shard_map/last_columns/pallas_call | solution.py:409
  200.5 1.0 copy.19
  (8 shorter events, 0.0 us)
Async XLA Ops:
  6.5 150.1 %all-gather.2.cloned.1.call-start = ((), (), s32[]{:S(2)}) async-start(), calls=%async_computation | async-start | bytes 4718592 | tf_op jit(solution)/shard_map/all_gather | solution.py:447
  18.1 67.7 %copy-start.1 = (bf16[1024,512]{1,0:T(8,128)(2,1)S(1)}, bf16[1024,512]{1,0:T(8,128)(2,1)}, u32[]{:S(2)}) copy-start(bf16[1024,512]{1,0:T(8,128)(2,1)} %gw.1) | copy-start | bytes 3145732
  18.2 67.7 %copy-start.2 = (bf16[1024,512]{1,0:T(8,128)(2,1)S(1)}, bf16[1024,512]{1,0:T(8,128)(2,1)}, u32[]{:S(2)}) copy-start(bf16[1024,512]{1,0:T(8,128)(2,1)} %gn.1) | copy-start | bytes 3145732
  18.2 67.7 %copy-start.5 = (f32[512]{0:T(512)S(1)}, f32[512]{0:T(512)}, u32[]{:S(2)}) copy-start(f32[512]{0:T(512)} %param.28) | copy-start | bytes 6148
  18.2 67.7 %copy-start.6 = (bf16[1024,512]{1,0:T(8,128)(2,1)S(1)}, bf16[1024,512]{1,0:T(8,128)(2,1)}, u32[]{:S(2)}) copy-start(bf16[1024,512]{1,0:T(8,128)(2,1)} %get-tuple-element.14.ow) | copy-start | bytes 3145732
  18.2 67.7 %copy-start.9 = (bf16[1024,128]{1,0:T(8,128)(2,1)S(1)}, bf16[1024,128]{1,0:T(8,128)(2,1)}, u32[]{:S(2)}) copy-start(bf16[1024,128]{1,0:T(8,128)(2,1)} %get-tuple-element.17.cn) | copy-start | bytes 786436
  85.9 1.2 copy-start.7
  87.2 1.0 copy-start.8
  88.2 11.1 %copy-start.3 = (bf16[256,1024]{1,0:T(8,128)(2,1)S(1)}, bf16[256,1024]{1,0:T(8,128)(2,1)}, u32[]{:S(2)}) copy-start(bf16[256,1024]{1,0:T(8,128)(2,1)} %shard.1) | copy-start | bytes 1572868
  88.2 11.1 %copy-start.4 = (f32[2048]{0:T(1024)S(1)}, f32[2048]{0:T(1024)}, u32[]{:S(2)}) copy-start(f32[2048]{0:T(1024)} %param.31) | copy-start | bytes 24580
  171.0 2.2 %copy-start = (bf16[1024,2048]{1,0:T(8,128)(2,1)S(1)}, bf16[1024,2048]{1,0:T(8,128)(2,1)}, u32[]{:S(2)}) copy-start(bf16[1024,2048]{1,0:T(8,128)(2,1)} %convolution_convert_fusion.partial) | copy-start | bytes 12582916
Sparse Core Ops, SparseCore 0:
  9.4 101.7 all-gather.1
